TPU v7x, 512 devices: a whole 4x4x16 slice. The times are simulated.
512 devices in a mesh: sp: 64 (over z, y), tp: 8 (over x, core).
Axes of the slice: x: 4, y: 4, z: 16, core: 2. Of those that a mesh axis runs over, the one named last changes fastest.
Arguments:
- tokens: bfloat16 [4096, 4, 2048], P(('sp', 'tp')), may hold values from -16 to 16
- norm_gain: float32 [2048], replicated, may hold values from 0.1 to 1.9
- w_query: bfloat16 [2048, 2048], P('sp', 'tp'), may hold values from -0.125 to 0.125
- w_forget: bfloat16 [2048, 2048], P('sp', 'tp'), may hold values from -0.125 to 0.125
- w_value: bfloat16 [2048, 2048], P('sp', 'tp'), may hold values from -0.125 to 0.125
- floor_gap: float32 [2048], P('tp'), may hold values from 0 to 0.15, as said below
- head_gain: float32 [2048], P('tp'), may hold values from 0.1 to 1.9
- w_out: bfloat16 [2048, 2048], P('tp', 'sp'), may hold values from -0.125 to 0.125
Outputs:
- mixed: bfloat16 [4096, 4, 2048], P(('sp', 'tp'))
Inputs may be any that keep to these rules, and one draw needn't show every extreme that they name: `floor_gap`: positive, at least 0.5 / 4096 and at most 0.15.
All inputs are finite; a program needn't handle non-finite values.
Results may differ from a plain program's by a relative error of at most 0.014.
Values may be sent and summed in bfloat16 or wider, within the bound.
No kernel may reach another device: no remote copies, remote signals or barrier semaphores. Data moves between devices by JAX's collectives and lax.ppermute only.
A program may use at most 128 MiB of HBM per device.

v0:
```python
import math

import jax
import jax.numpy as jnp
from jax import lax
from jax.sharding import Mesh
from jax.sharding import PartitionSpec as P

KEY_DIM = 128
VAL_DIM = 128
SP = ("sp_0", "sp_1")
SP_TP = ("sp_0", "sp_1", "tp")


eps_norm = 1e-06


def sent_together(arrays, axis, dim, along):
    ends, at = ([], 0)
    for a in arrays[:-1]:
        at += a.shape[along]
        ends.append(at)
    both = jnp.concatenate(arrays, axis=along)
    return tuple(jnp.split(lax.all_gather(both, axis, axis=dim, tiled=True), ends, axis=along))


def copy_for_each(value, axis):
    length = lax.axis_size(axis)
    return lax.all_to_all(
        jnp.broadcast_to(value[None], (length, *value.shape)), axis, 0, 0, tiled=True
    )


def joined_along(pieces, dim):
    lengths = list(pieces.shape[1:])
    lengths[dim] *= pieces.shape[0]
    return jnp.moveaxis(pieces, 0, dim).reshape(lengths)


def gather_directly(value, axis, dim):
    pieces = copy_for_each(value, axis)
    return joined_along(pieces, dim)


def filled_with(value, identity):
    return jax.tree.map(
        lambda part, zero: jnp.zeros_like(part) + jnp.asarray(zero, part.dtype), value, identity
    )


def prefix_by_axis(value, axes, combine, identity):
    before = start = filled_with(value, identity)
    so_far = value
    for axis in reversed(axes):
        length, mine = (lax.axis_size(axis), lax.axis_index(axis))
        pieces = jax.tree.map(lambda part: lax.all_gather(part, axis), so_far)
        inside, so_far = (start, start)
        for k in range(length):
            passed = k < mine
            so_far = combine(so_far, jax.tree.map(lambda part: part[k], pieces))
            inside = jax.tree.map(lambda new, old: jnp.where(passed, new, old), so_far, inside)
        before = combine(inside, before)
    return before


def whole_of(value, axes, dim):
    if not axes:
        return value
    nearer = lax.all_gather(value, axes[-1], axis=dim, tiled=True)
    return whole_of(nearer, axes[:-1], dim)


def in_blocks(value, dim, length):
    lengths = value.shape
    pieces = value.reshape(*lengths[:dim], length, lengths[dim] // length, *lengths[dim + 1 :])
    return jnp.moveaxis(pieces, dim, 0)


def summed_on_arrival(value, axis, dim):
    pieces = in_blocks(value, dim, lax.axis_size(axis))
    arrived = lax.all_to_all(pieces, axis, split_axis=0, concat_axis=0, tiled=True)
    return arrived.astype(jnp.float32).sum(axis=0)


def link_states(earlier, later):
    decay_early, state_early = earlier
    decay_late, state_late = later
    return (decay_early * decay_late, decay_late[..., None] * state_early + state_late)


def local_pass(query, inkey, log_forget, values):
    block_len = query.shape[1]
    cumulative = jnp.cumsum(log_forget, axis=1)
    final = cumulative[:, -1]
    query_scaled = query * jnp.exp(cumulative)
    key_scaled = inkey * jnp.exp(-cumulative)
    key_final = inkey * jnp.exp(final[:, None] - cumulative)
    scores = jnp.einsum("ntshk,nushk->nshtu", query_scaled, key_scaled)
    positions = lax.iota(jnp.int32, block_len)
    causal = positions[:, None] >= positions[None, :]
    scores = jnp.where(causal, scores, 0.0)
    inside = jnp.einsum("nshtu,nushv->ntshv", scores, values)
    updates = jnp.einsum("nushk,nushv->nshkv", key_final, values)
    block_decay = jnp.exp(final)

    def advance(carry, inputs):
        decay_block, update_block = inputs
        return (decay_block[..., None] * carry + update_block, carry)

    end_state, entering = lax.scan(advance, jnp.zeros_like(updates[0]), (block_decay, updates))
    inside = inside + jnp.einsum("ntshk,nshkv->ntshv", query_scaled, entering)
    offsets = jnp.cumsum(final, axis=0) - final
    reach = query_scaled * jnp.exp(offsets)[:, None]
    total_decay = jnp.exp(jnp.sum(final, axis=0))
    return (inside, reach, total_decay, end_state)


def read_out(reach, incoming):
    return jnp.einsum("ntshk,shkv->ntshv", reach, incoming)


def body(tokens, norm_gain, w_query, w_forget, w_value, floor_gap, head_gain, w_out):
    flat = tokens.astype(jnp.float32)
    scale = lax.rsqrt(jnp.mean(flat * flat, axis=-1, keepdims=True) + eps_norm)
    normed = (flat * scale * norm_gain).astype(jnp.bfloat16)
    whole_query, whole_forget, whole_value = sent_together((w_query, w_forget, w_value), SP, 0, 1)
    key_width = whole_query.shape[1]
    piece = gather_directly(normed, "tp", 0)
    flat_rows = piece.reshape(-1, piece.shape[-1])
    outputs = [
        jnp.dot(flat_rows, weight, preferred_element_type=jnp.float32).astype(jnp.bfloat16)
        for weight in (whole_query, whole_forget, whole_value)
    ]
    joined = jnp.concatenate(outputs, axis=1)
    projected = joined.reshape(piece.shape[0], piece.shape[1], joined.shape[1])
    projected = lax.optimization_barrier(projected).astype(jnp.float32)
    positions_dev, sequences = (projected.shape[0], projected.shape[1])
    head_count = key_width // KEY_DIM
    block_len = math.gcd(positions_dev, 128)
    block_count = positions_dev // block_len

    def blocks(value, channels):
        return value.reshape(block_count, block_len, sequences, head_count, channels)

    query = jax.nn.silu(blocks(projected[..., :key_width], KEY_DIM))
    inkey = floor_gap.reshape(head_count, KEY_DIM) * jax.nn.sigmoid(
        -blocks(projected[..., key_width : 2 * key_width], KEY_DIM)
    )
    log_forget = jnp.log1p(-inkey)
    values = blocks(projected[..., 2 * key_width :], VAL_DIM)
    inside, reach, total_decay, end_state = local_pass(query, inkey, log_forget, values)
    _, incoming = prefix_by_axis(
        (total_decay, end_state),
        SP,
        link_states,
        (jnp.ones_like(total_decay), jnp.zeros_like(end_state)),
    )
    recurrent = inside + read_out(reach, incoming)
    mean_square = jnp.mean(recurrent * recurrent, axis=-1, keepdims=True)
    hidden = recurrent * lax.rsqrt(mean_square + eps_norm) * head_gain.reshape(head_count, VAL_DIM)
    hidden = hidden.astype(jnp.bfloat16).reshape(positions_dev, sequences, head_count * VAL_DIM)
    out_columns = whole_of(w_out, SP, 1)
    piece = hidden
    summed = summed_on_arrival(
        jnp.einsum("psh,hd->psd", piece, out_columns, preferred_element_type=jnp.float32).astype(
            jnp.bfloat16
        ),
        "tp",
        0,
    )
    return summed.astype(jnp.bfloat16)


def solution(mesh):
    finer = Mesh(mesh.devices.reshape(16, 4, mesh.shape["tp"]), ("sp_0", "sp_1", "tp"))
    in_specs = (
        P(SP_TP, None, None),
        P(),
        P(SP, "tp"),
        P(SP, "tp"),
        P(SP, "tp"),
        P("tp"),
        P("tp"),
        P("tp", SP),
    )
    out_specs = P(SP_TP, None, None)
    return jax.shard_map(body, mesh=finer, in_specs=in_specs, out_specs=out_specs, check_vma=False)
```

profile of v0, /device:TPU:1, one launch (start us, length us, event | category | flops | bytes accessed | tf_op | source)
XLA Modules:
  0.0 410.2 jit_solution(15214919342758421356)
XLA Ops:
  6.5 1.4 pad_maximum_fusion.1
  7.9 0.0 all-gather.7.cloned.1.call-update
  7.9 0.0 all-gather.13.cloned.1.call-start
  8.0 1.1 fusion.91
  9.1 1.0 fusion.93
  10.1 0.5 broadcast_in_dim.19
  10.6 24.2 %all_to_all.10 = bf16[8,8,4,2048]{3,2,1,0:T(4,128)(2,1)S(1)} all-to-all(bf16[8,8,4,2048]{3,2,1,0:T(4,128)(2,1)S(1)} %broadcast_in_dim.19), channel_id=1, replica_groups=mesh['sp_0'=16,'sp_1'=4,'tp'=8] {'tp'}, dimensions={0} | all-to-all | bytes 2097152 | tf_op jit(solution)/shard_map/all_to_all | solution.py:29
  34.8 0.3 reshape_reshape.3
  35.1 115.0 %all-gather.7.cloned.1.call-done = bf16[2048,768]{1,0:T(8,128)(2,1)} async-done(((bf16[32,768]{1,0:T(8,128)(2,1)}), bf16[2048,768]{1,0:T(8,128)(2,1)}) %all-gather.7.cloned.1.call-update) | async-done | bytes 3145744 | tf_op jit(solution)/shard_map/all_gather | solution.py:24
  150.0 1.8 convolution_convert_fusion.1
  151.8 1.8 convolution_convert_fusion.2
  153.6 1.8 convolution_convert_fusion.3
  155.4 0.2 copy.100
  155.6 0.1 reshape.227
  155.7 0.1 convert_element_type.31
  155.7 0.1 fusion.95
  155.9 0.2 reshape.256
  156.1 0.2 div.47
  156.3 0.0 copy-start
  156.4 0.4 fusion.128
  156.8 0.1 reshape.254
  156.9 1.2 convolution_add_fusion
  158.1 0.0 all-gather.13.cloned.1.call-update
  158.1 0.0 all-gather.9.cloned.1.call-start
  158.2 9.1 %all-gather = f32[4,1,4,2,128]{4,2,3,1,0:T(4,128)S(1)} all-gather(f32[1,1,4,2,128]{4,2,3,1,0:T(4,128)S(1)} %get-tuple-element.44), channel_id=2, replica_groups=mesh['sp_0'=16,'sp_1'=4,'tp'=8] {'sp_1'}, dimensions={0}, use_global_device_ids=true | all-gather | bytes 20480 | tf_op jit(solution)/shard_map/all_gather | solution.py:56
  167.4 33.2 %all-gather.13.cloned.1.call-done = f32[16,2,128,128]{3,2,1,0:T(8,128)} async-done(((f32[4,2,128,128]{3,2,1,0:T(8,128)}), f32[16,2,128,128]{3,2,1,0:T(8,128)}) %all-gather.13.cloned.1.call-update) | async-done | bytes 2097168 | tf_op jit(solution)/shard_map/all_gather | solution.py:56
  200.5 2.6 bitcast_add_fusion
  203.2 0.0 all-gather.9.cloned.1.call-update
  203.2 0.0 all-gather.11.cloned.1.call-start
  203.2 9.0 %all_gather.30 = bf16[256,128]{0,1:T(8,128)(2,1)S(1)} all-gather(bf16[256,32]{0,1:T(8,128)(2,1)S(1)} %copy-done), channel_id=1, replica_groups=mesh['sp_0'=16,'sp_1'=4,'tp'=8] {'sp_1'}, dimensions={1}, use_global_device_ids=true | all-gather | bytes 81920 | tf_op jit(solution)/shard_map/all_gather | solution.py:69
  212.2 0.7 copy.140
  212.9 0.0 all-gather.11.cloned.1.call-update
  213.1 0.2 reshape.255
  213.3 26.6 %all_gather.27 = f32[16,4,2,128]{3,1,2,0:T(4,128)S(1)} all-gather(f32[1,4,2,128]{3,1,2,0:T(4,128)S(1)} %get-tuple-element.38), channel_id=1, replica_groups=mesh['sp_0'=16,'sp_1'=4,'tp'=8] {'sp_0'}, dimensions={0}, use_global_device_ids=true | all-gather | bytes 69632 | tf_op jit(solution)/shard_map/all_gather | solution.py:56
  240.1 0.4 fusion.2
  240.5 0.2 fusion.1
  240.7 0.0 copy-start.2
  240.7 69.2 %all-gather.9.cloned.1.call-done = f32[16,4,2,128,128]{4,3,2,1,0:T(8,128)} async-done(((f32[1,4,2,128,128]{4,3,2,1,0:T(8,128)}), f32[16,4,2,128,128]{4,3,2,1,0:T(8,128)}) %all-gather.9.cloned.1.call-update) | async-done | bytes 8388624 | tf_op jit(solution)/shard_map/all_gather | solution.py:56
  309.9 8.7 %multiply_reduce_fusion = (f32[64,4,2]{0,2,1:T(2,128)S(1)}, f32[1,64,4,2,128]{4,1,3,2,0:T(8,128)S(1)}) fusion(f32[1,64,4,2,128]{4,1,3,2,0:T(8,128)S(1)} %fusion.1, f32[4,2,128]{2,1,0:T(2,128)S(1)} %copy.138, f32[1,64,4,2,128]{4,3,2,1,0:T(2,128)S(1)} %fusion.128, f32[64,4,2,128]{3,2,1,0:T(2,128)S(1)} %reshape.255, ...), kind=kOutput, calls=%fused_computation.122 | convolution fusion | flops 25230848 | bytes 11626516 | tf_op jit(solution)/shard_map/ntshk,shkv->ntshv/dot_general | solution.py:119
  318.6 0.1 multiply_convert_fusion
  318.7 0.1 copy.139
  318.9 0.1 reshape.230
  319.0 50.7 %all-gather.11.cloned.1.call-done = bf16[256,2048]{1,0:T(8,128)(2,1)} async-done(((bf16[256,128]{1,0:T(8,128)(2,1)}), bf16[256,2048]{1,0:T(8,128)(2,1)}) %all-gather.11.cloned.1.call-update) | async-done | bytes 1048592 | tf_op jit(solution)/shard_map/all_gather | solution.py:69
  369.7 1.7 fusion
  371.3 0.1 copy.141
  371.5 31.3 %all_to_all.11 = bf16[8,8,4,2048]{3,1,2,0:T(8,128)(2,1)S(1)} all-to-all(bf16[8,8,4,2048]{3,1,2,0:T(8,128)(2,1)S(1)} %copy.141), channel_id=1, replica_groups=mesh['sp_0'=16,'sp_1'=4,'tp'=8] {'tp'}, dimensions={0} | all-to-all | bytes 2097152 | tf_op jit(solution)/shard_map/all_to_all | solution.py:81
  402.7 0.1 reduce_sum.36
  402.9 0.8 copy.143
  (41 shorter events, 0.3 us)
Async XLA Ops:
  6.5 143.5 %all-gather.7.cloned.1.call-start = ((), (), s32[]{:S(2)}) async-start(), calls=%async_computation.2 | async-start | bytes 3194880 | tf_op jit(solution)/shard_map/all_gather | solution.py:24
  7.9 192.6 %all-gather.13.cloned.1.call-start = ((), (), s32[]{:S(2)}) async-start(), calls=%async_computation.5 | async-start | bytes 2621440 | tf_op jit(solution)/shard_map/all_gather | solution.py:56
  155.4 1.0 copy-start.1
  156.3 46.9 %copy-start = (bf16[256,32]{0,1:T(8,128)(2,1)S(1)}, bf16[256,32]{0,1:T(8,128)(2,1)}, u32[]{:S(2)}) copy-start(bf16[256,32]{0,1:T(8,128)(2,1)} %param.15) | copy-start | bytes 49156
  158.1 151.8 %all-gather.9.cloned.1.call-start = ((), (), s32[]{:S(2)}) async-start(), calls=%async_computation.3 | async-start | bytes 8912896 | tf_op jit(solution)/shard_map/all_gather | solution.py:56
  203.2 166.5 %all-gather.11.cloned.1.call-start = ((), (), s32[]{:S(2)}) async-start(), calls=%async_computation.4 | async-start | bytes 1114112 | tf_op jit(solution)/shard_map/all_gather | solution.py:69
  240.7 77.9 %copy-start.2 = (f32[256]{0:T(256)S(1)}, f32[256]{0:T(256)}, u32[]{:S(2)}) copy-start(f32[256]{0:T(256)} %param.14) | copy-start | bytes 3076
Sparse Core Ops, SparseCore 0:
  10.3 139.7 all-gather.6
  158.2 42.2 all-gather.12
  203.3 106.5 all-gather.8
  311.8 57.8 all-gather.10
where the time goes:
time: 411 us; the launch traced here: 410 us
  waiting for transfers between devices  268 us (65%)
  blocking collectives  100 us (24%)
  matrix products  17.4 us (4%)
  between operations  13.6 us (3%)
  other arithmetic  7.07 us (2%)
    all_gather x1, waiting for transfers between devices, sent_together(): lax.all_gather(both, axis, axis=dim, tiled=True)  115 us
    all_gather x2, waiting for transfers between devices, prefix_by_axis(): pieces = jax.tree.map(lambda part: lax.all_gather(part, axis), so_far)  102 us
    all_gather x1, waiting for transfers between devices, whole_of(): nearer = lax.all_gather(value, axes[-1], axis=dim, tiled=True)  50.7 us
    all_gather x2, blocking collectives, prefix_by_axis(): pieces = jax.tree.map(lambda part: lax.all_gather(part, axis), so_far)  35.7 us
    all_to_all x1, blocking collectives, summed_on_arrival(): lax.all_to_all(pieces, axis, split_axis=0, concat_axis=0, tiled=True)  31.3 us
    all_to_all x1, blocking collectives, copy_for_each(): lax.all_to_all(jnp.broadcast_to(value[None], (length, *value.shape)), axi...  24.2 us
    all_gather x1, blocking collectives, whole_of(): nearer = lax.all_gather(value, axes[-1], axis=dim, tiled=True)  8.98 us
    dot_general x1, matrix products, read_out(): return jnp.einsum('ntshk,shkv->ntshv', reach, incoming)  8.66 us
  transfers between devices with their start and end apart: 4, of which 4 were waited for; matrix products, arithmetic and copies ran while one was open for 3% of the time, Pallas kernels for 0%

commit v1 on v0

v1 whole, which is shorter than its diff:
```python
import math

import jax
import jax.numpy as jnp
from jax import lax
from jax.sharding import Mesh
from jax.sharding import PartitionSpec as P

KEY_DIM = 128
VAL_DIM = 128
YT = ("y", "tp")

eps_norm = 1e-06


def exchanged(value, axis):
    return lax.all_to_all(value, axis, 0, 0, tiled=True)


def copies(value, count):
    return jnp.broadcast_to(value[None], (count, *value.shape))


def split_two(value):
    high = value.astype(jnp.bfloat16)
    low = (value - high.astype(jnp.float32)).astype(jnp.bfloat16)
    return high, low


def body(tokens, norm_gain, w_query, w_forget, w_value, floor_gap, head_gain, w_out):
    nz, ny, nt = (lax.axis_size(a) for a in ("z", "y", "tp"))
    pos, seqs, width = tokens.shape
    chunk = w_query.shape[0]
    key_width = w_query.shape[1]
    heads = key_width // KEY_DIM
    stretch = pos * ny * nt
    part = nz * chunk

    out_z = exchanged(copies(w_out, nz), "z")
    out_z = out_z.transpose(1, 0, 2).reshape(key_width, part)

    flat = tokens.astype(jnp.float32)
    scale = lax.rsqrt(jnp.mean(flat * flat, axis=-1, keepdims=True) + eps_norm)
    normed = (flat * scale * norm_gain).astype(jnp.bfloat16)
    by_y = normed.reshape(pos, seqs, nz, ny, chunk).transpose(3, 1, 0, 2, 4).reshape(ny, seqs, pos, part)
    send = jnp.broadcast_to(by_y[:, None], (ny, nt, seqs, pos, part)).reshape(ny * nt, seqs, pos, part)
    rows = exchanged(send, YT)

    weights = jnp.concatenate((w_forget, w_value, w_query), axis=1)
    weights = lax.all_gather(weights, "z", axis=0, tiled=True)
    rows = rows.transpose(1, 0, 2, 3).reshape(seqs, stretch, part)
    partial = jnp.einsum("sph,hd->spd", rows, weights, preferred_element_type=jnp.float32).astype(jnp.bfloat16)
    fv = exchanged(partial[..., : 2 * key_width], "y").astype(jnp.float32).sum(axis=0)
    fv = fv.astype(jnp.bfloat16)
    later = jnp.concatenate((partial[..., 2 * key_width :], copies(out_z, ny)), axis=2)
    later = exchanged(later, "y")
    query = later[..., :key_width].astype(jnp.float32).sum(axis=0).astype(jnp.bfloat16)
    out_rows = later[..., key_width:]

    forget = fv[:, :key_width].astype(jnp.float32)
    values = fv[:, key_width:].reshape(stretch, heads, VAL_DIM)
    inkey = floor_gap * jax.nn.sigmoid(-forget)
    log_forget = jnp.log1p(-inkey)
    positions = lax.iota(jnp.int32, stretch)
    causal = positions[:, None] >= positions[None, :]
    cumulative = jnp.dot(causal.astype(jnp.float32), log_forget, precision=lax.Precision.HIGHEST)
    final = cumulative[-1]
    key_final = (inkey * jnp.exp(final - cumulative)).astype(jnp.bfloat16).reshape(stretch, heads, KEY_DIM)
    end_state = jnp.einsum("uhk,uhv->hkv", key_final, values, preferred_element_type=jnp.float32)
    decay = jnp.exp(final)

    mine = heads * KEY_DIM // nz
    high, low = split_two(decay.reshape(nz, mine, 1))
    pieces = jnp.concatenate(
        (
            end_state.astype(jnp.bfloat16).reshape(nz, mine, VAL_DIM),
            jnp.broadcast_to(high, (nz, mine, 64)),
            jnp.broadcast_to(low, (nz, mine, 64)),
        ),
        axis=2,
    )
    pieces = exchanged(pieces, "z").astype(jnp.float32)
    state = jnp.zeros((mine, VAL_DIM), jnp.float32)
    entering = []
    for k in range(nz):
        entering.append(state.astype(jnp.bfloat16))
        factor = pieces[k, :, VAL_DIM : VAL_DIM + 1] + pieces[k, :, VAL_DIM + 64 : VAL_DIM + 65]
        state = factor * state + pieces[k, :, :VAL_DIM]
    incoming = exchanged(jnp.stack(entering), "z").reshape(heads, KEY_DIM, VAL_DIM)

    query = jax.nn.silu(query.astype(jnp.float32))
    query_scaled = (query * jnp.exp(cumulative)).astype(jnp.bfloat16).reshape(stretch, heads, KEY_DIM)
    key_scaled = (inkey * jnp.exp(-cumulative)).astype(jnp.bfloat16).reshape(stretch, heads, KEY_DIM)
    scores = jnp.einsum("thk,uhk->htu", query_scaled, key_scaled, preferred_element_type=jnp.float32)
    scores = jnp.where(causal, scores, 0.0).astype(jnp.bfloat16)
    recurrent = jnp.einsum("htu,uhv->thv", scores, values, preferred_element_type=jnp.float32)
    recurrent = recurrent + jnp.einsum("thk,hkv->thv", query_scaled, incoming, preferred_element_type=jnp.float32)
    mean_square = jnp.mean(recurrent * recurrent, axis=-1, keepdims=True)
    hidden = recurrent * lax.rsqrt(mean_square + eps_norm) * head_gain.reshape(heads, VAL_DIM)
    hidden = hidden.astype(jnp.bfloat16).reshape(stretch, heads * VAL_DIM)

    mixed = jnp.einsum("ph,yhd->pyd", hidden, out_rows, preferred_element_type=jnp.float32).astype(jnp.bfloat16)
    mixed = exchanged(mixed.reshape(ny * nt, pos, width), YT)
    mixed = mixed.reshape(seqs, nt, pos, width).astype(jnp.float32).sum(axis=1).astype(jnp.bfloat16)
    mixed = mixed.reshape(seqs, pos, ny, nz, chunk).transpose(1, 0, 3, 2, 4)
    return mixed.reshape(pos, seqs, width)


def solution(mesh):
    finer = Mesh(mesh.devices.reshape(16, 4, mesh.shape["tp"]), ("z", "y", "tp"))
    sp = ("z", "y")
    in_specs = (
        P(("z", "y", "tp"), None, None),
        P(),
        P(sp, "tp"),
        P(sp, "tp"),
        P(sp, "tp"),
        P("tp"),
        P("tp"),
        P("tp", sp),
    )
    out_specs = P(("z", "y", "tp"), None, None)
    return jax.shard_map(body, mesh=finer, in_specs=in_specs, out_specs=out_specs, check_vma=False)
```

time: 411 us -> 200 us (0.49)
  waiting for transfers between devices: 268 us -> 41 us
  starting transfers between devices: 0.13 us -> 34.9 us
  matrix products: 17.4 us -> 2.71 us
  between operations: 13.6 us -> 0.38 us
  other arithmetic: 7.07 us -> 15.6 us
  local copies, waits for them, and re-layouts: 3.67 us -> 9.05 us
  blocking collectives: 100 us -> 95.8 us
    all_gather x4 -> x0, waiting for transfers between devices: 268 us -> none  [the longest x1 115 us: sent_together(): lax.all_gather(both, axis, axis=dim, tiled=True)]
    all_to_all x0 -> x5, waiting for transfers between devices: none -> 41 us  [exchanged(): return lax.all_to_all(value, axis, 0, 0, tiled=True)]
    all_to_all x0 -> x5, starting transfers between devices: none -> 34.9 us  [exchanged(): return lax.all_to_all(value, axis, 0, 0, tiled=True)]
    dot_general x8 -> x6, matrix products: 17.4 us -> 2.71 us  [the longest x1 0.99 us: body(): jnp.einsum('sph,hd->spd', rows, weights, preferred_element_type=jnp.float32)]
    unnamed x0 -> x14, other arithmetic: none -> 9.3 us
    all_gather x3 -> x1, blocking collectives: 44.7 us -> 36.3 us  [body(): weights = lax.all_gather(weights, 'z', axis=0, tiled=True)]
  transfers between devices with their start and end apart: 4 -> 5, of which waited for: 4 -> 4; matrix products, arithmetic and copies ran while one was open for 3% -> 3% of each run, Pallas kernels for 0% -> 0%
where the time goes in v1:
time: 200 us; the launch traced here: 199 us
  blocking collectives  95.8 us (48%)
  waiting for transfers between devices  41 us (20%)
  starting transfers between devices  34.9 us (17%)
  other arithmetic  15.6 us (8%)
  local copies, waits for them, and re-layouts  9.05 us (5%)
  matrix products  2.71 us (1%)
    all_to_all x2, blocking collectives, exchanged(): return lax.all_to_all(value, axis, 0, 0, tiled=True)  59.5 us
    all_to_all x5, waiting for transfers between devices, exchanged(): return lax.all_to_all(value, axis, 0, 0, tiled=True)  41 us
    all_gather x1, blocking collectives, body(): weights = lax.all_gather(weights, 'z', axis=0, tiled=True)  36.3 us
    all_to_all x5, starting transfers between devices, exchanged(): return lax.all_to_all(value, axis, 0, 0, tiled=True)  34.9 us
    unnamed x14, other arithmetic  9.3 us
  transfers between devices with their start and end apart: 5, of which 4 were waited for; matrix products, arithmetic and copies ran while one was open for 3% of the time, Pallas kernels for 0%

profile of v1, /device:TPU:1, one launch (start us, length us, event | category | flops | bytes accessed | tf_op | source)
XLA Modules:
  0.0 199.4 jit_solution(15762389516083528278)
XLA Ops:
  0.0 1.1 fusion.7
  1.1 1.0 fusion.9
  2.1 0.3 reshape.1079
  2.5 0.4 broadcast_in_dim.22
  3.1 26.8 %all_to_all.35 = bf16[32,4,8,512]{3,2,1,0:T(8,128)(2,1)S(1)} all-to-all(bf16[32,4,8,512]{3,2,1,0:T(8,128)(2,1)S(1)} %bitcast.42), channel_id=1, replica_groups=mesh['z'=16,'y'=4,'tp'=8] {'y','tp'}, dimensions={0} | all-to-all | bytes 2097152 | tf_op jit(solution)/shard_map/all_to_all | solution.py:17
  29.9 0.7 broadcast_in_dim.50
  30.7 13.7 %all-to-all-start.2 = ((bf16[16,256,32]{1,2,0:T(8,128)(2,1)}), bf16[16,256,32]{1,2,0:T(8,128)(2,1)S(1)}, u32[]{:S(2)}, u32[]{:S(2)}) async-start(bf16[16,256,32]{1,2,0:T(8,128)(2,1)} %broadcast_in_dim.50), calls=%async_computation.2 | async-start | bytes 524288 | tf_op jit(solution)/shard_map/all_to_all | solution.py:17
  44.4 36.3 %all_gather.3 = bf16[512,768]{1,0:T(8,128)(2,1)S(1)} all-gather(bf16[32,768]{1,0:T(8,128)(2,1)S(1)} %pad_maximum_fusion.2), channel_id=1, replica_groups=mesh['z'=16,'y'=4,'tp'=8] {'z'}, dimensions={0}, use_global_device_ids=true | all-gather | bytes 835584 | tf_op jit(solution)/shard_map/all_gather | solution.py:50
  80.7 1.0 convolution_convert_fusion
  81.7 1.1 slice.208
  82.9 3.5 %all-to-all-start.1 = ((bf16[4,256,512]{2,1,0:T(8,128)(2,1)}), bf16[4,256,512]{2,1,0:T(8,128)(2,1)S(1)}, u32[]{:S(2)}, u32[]{:S(2)}) async-start(bf16[4,256,512]{2,1,0:T(8,128)(2,1)} %slice.208), calls=%async_computation.1 | async-start | bytes 2097152 | tf_op jit(solution)/shard_map/all_to_all | solution.py:17
  86.6 0.9 slice-done
  87.6 1.3 pad_maximum_fusion
  88.8 7.2 %all-to-all-done.1 = bf16[4,256,512]{2,1,0:T(8,128)(2,1)S(1)} async-done(((bf16[4,256,512]{2,1,0:T(8,128)(2,1)}), bf16[4,256,512]{2,1,0:T(8,128)(2,1)S(1)}, u32[]{:S(2)}, u32[]{:S(2)}) %all-to-all-start.1) | async-done | bytes 1048608 | tf_op jit(solution)/shard_map/all_to_all | solution.py:17
  96.1 3.6 %all-to-all-start.3 = ((bf16[4,256,768]{2,1,0:T(8,128)(2,1)}), bf16[4,256,768]{2,1,0:T(8,128)(2,1)S(1)}, u32[]{:S(2)}, u32[]{:S(2)}) async-start(bf16[4,256,768]{2,1,0:T(8,128)(2,1)} %pad_maximum_fusion), calls=%async_computation.3 | async-start | bytes 3145728 | tf_op jit(solution)/shard_map/all_to_all | solution.py:17
  100.3 0.4 fusion.15
  101.1 11.3 %all-to-all-done.3 = bf16[4,256,768]{2,1,0:T(8,128)(2,1)S(1)} async-done(((bf16[4,256,768]{2,1,0:T(8,128)(2,1)}), bf16[4,256,768]{2,1,0:T(8,128)(2,1)S(1)}, u32[]{:S(2)}, u32[]{:S(2)}) %all-to-all-start.3) | async-done | bytes 1572896 | tf_op jit(solution)/shard_map/all_to_all | solution.py:17
  112.5 0.3 multiply_convert_fusion.1
  113.2 0.7 pad_maximum_fusion.1
  114.0 10.4 %all-to-all-start.4 = ((bf16[16,16,256]{2,1,0:T(8,128)(2,1)}), bf16[16,16,256]{2,1,0:T(8,128)(2,1)S(1)}, u32[]{:S(2)}, u32[]{:S(2)}) async-start(bf16[16,16,256]{2,1,0:T(8,128)(2,1)} %pad_maximum_fusion.1), calls=%async_computation.4 | async-start | bytes 262144 | tf_op jit(solution)/shard_map/all_to_all | solution.py:17
  124.3 0.6 constant_dynamic-update-slice_fusion.15
  124.9 11.4 %all-to-all-done.4 = bf16[16,16,256]{2,1,0:T(8,128)(2,1)S(1)} async-done(((bf16[16,16,256]{2,1,0:T(8,128)(2,1)}), bf16[16,16,256]{2,1,0:T(8,128)(2,1)S(1)}, u32[]{:S(2)}, u32[]{:S(2)}) %all-to-all-start.4) | async-done | bytes 131104 | tf_op jit(solution)/shard_map/all_to_all | solution.py:17
  136.3 0.3 fusion.22
  136.6 0.3 fusion.21
  136.9 0.7 constant_dynamic-update-slice_fusion.14
  137.6 0.7 constant_dynamic-update-slice_fusion.13
  138.3 0.7 constant_dynamic-update-slice_fusion.12
  138.9 0.7 constant_dynamic-update-slice_fusion.11
  139.6 0.7 constant_dynamic-update-slice_fusion.10
  140.2 0.7 constant_dynamic-update-slice_fusion.9
  140.9 0.7 constant_dynamic-update-slice_fusion.8
  141.6 0.7 constant_dynamic-update-slice_fusion.7
  142.2 0.7 constant_dynamic-update-slice_fusion.6
  142.9 0.7 constant_dynamic-update-slice_fusion.5
  143.6 0.7 constant_dynamic-update-slice_fusion.4
  144.2 0.7 constant_dynamic-update-slice_fusion.3
  144.9 0.7 constant_dynamic-update-slice_fusion.2
  145.6 0.7 constant_dynamic-update-slice_fusion.1
  146.2 0.7 constant_dynamic-update-slice_fusion
  146.9 3.8 %all-to-all-start.5 = ((bf16[16,16,128]{2,1,0:T(8,128)(2,1)}), bf16[16,16,128]{2,1,0:T(8,128)(2,1)S(1)}, u32[]{:S(2)}, u32[]{:S(2)}) async-start(bf16[16,16,128]{2,1,0:T(8,128)(2,1)} %constant_dynamic-update-slice_fusion), calls=%async_computation.5 | async-start | bytes 131072 | tf_op jit(solution)/shard_map/all_to_all | solution.py:17
  150.7 0.4 fusion.1
  151.1 11.1 %all-to-all-done.5 = bf16[16,16,128]{2,1,0:T(8,128)(2,1)S(1)} async-done(((bf16[16,16,128]{2,1,0:T(8,128)(2,1)}), bf16[16,16,128]{2,1,0:T(8,128)(2,1)S(1)}, u32[]{:S(2)}, u32[]{:S(2)}) %all-to-all-start.5) | async-done | bytes 65568 | tf_op jit(solution)/shard_map/all_to_all | solution.py:17
  162.6 0.5 convolution_convert_fusion.1
  163.1 0.8 copy.46
  163.9 0.8 reshape.1089
  164.7 32.7 %all_to_all.36 = bf16[32,8,2048]{2,1,0:T(8,128)(2,1)S(1)} all-to-all(bf16[32,8,2048]{2,1,0:T(8,128)(2,1)S(1)} %reshape.1089), channel_id=1, replica_groups=mesh['z'=16,'y'=4,'tp'=8] {'y','tp'}, dimensions={0} | all-to-all | bytes 2097152 | tf_op jit(solution)/shard_map/all_to_all | solution.py:17
  197.5 0.4 reshape.1091
  198.2 1.2 reshape.1095
  (41 shorter events, 2.8 us)
Async XLA Ops:
  3.0 27.0 %copy-start.1 = (bf16[256,32]{0,1:T(8,128)(2,1)S(1)}, bf16[256,32]{0,1:T(8,128)(2,1)}, u32[]{:S(2)}) copy-start(bf16[256,32]{0,1:T(8,128)(2,1)} %param.15) | copy-start | bytes 49156
  3.1 41.3 %copy-start.2 = (bf16[32,256]{1,0:T(8,128)(2,1)S(1)}, bf16[32,256]{1,0:T(8,128)(2,1)}, u32[]{:S(2)}) copy-start(bf16[32,256]{1,0:T(8,128)(2,1)} %param.10) | copy-start | bytes 49156
  3.1 41.2 %copy-start.3 = (bf16[32,256]{1,0:T(8,128)(2,1)S(1)}, bf16[32,256]{1,0:T(8,128)(2,1)}, u32[]{:S(2)}) copy-start(bf16[32,256]{1,0:T(8,128)(2,1)} %param.12) | copy-start | bytes 49156
  3.1 41.2 %copy-start.4 = (bf16[32,256]{1,0:T(8,128)(2,1)S(1)}, bf16[32,256]{1,0:T(8,128)(2,1)}, u32[]{:S(2)}) copy-start(bf16[32,256]{1,0:T(8,128)(2,1)} %param.11) | copy-start | bytes 49156
  30.7 52.2 %all-to-all-start.2 = ((bf16[16,256,32]{1,2,0:T(8,128)(2,1)}), bf16[16,256,32]{1,2,0:T(8,128)(2,1)S(1)}, u32[]{:S(2)}, u32[]{:S(2)}) async-start(bf16[16,256,32]{1,2,0:T(8,128)(2,1)} %broadcast_in_dim.50), calls=%async_computation.2 | async-start | bytes 524288 | tf_op jit(solution)/shard_map/all_to_all | solution.py:17
  81.7 4.8 %copy-start = (bf16[4,256,768]{2,1,0:T(8,128)(2,1)}, bf16[4,256,768]{2,1,0:T(8,128)(2,1)S(1)}, u32[]{:S(2)}) copy-start(bf16[4,256,768]{2,1,0:T(8,128)(2,1)S(1)} %convolution_convert_fusion) | copy-start | bytes 4718596
  82.9 13.2 %all-to-all-start.1 = ((bf16[4,256,512]{2,1,0:T(8,128)(2,1)}), bf16[4,256,512]{2,1,0:T(8,128)(2,1)S(1)}, u32[]{:S(2)}, u32[]{:S(2)}) async-start(bf16[4,256,512]{2,1,0:T(8,128)(2,1)} %slice.208), calls=%async_computation.1 | async-start | bytes 2097152 | tf_op jit(solution)/shard_map/all_to_all | solution.py:17
  86.5 1.0 slice-start
  96.1 16.3 %all-to-all-start.3 = ((bf16[4,256,768]{2,1,0:T(8,128)(2,1)}), bf16[4,256,768]{2,1,0:T(8,128)(2,1)S(1)}, u32[]{:S(2)}, u32[]{:S(2)}) async-start(bf16[4,256,768]{2,1,0:T(8,128)(2,1)} %pad_maximum_fusion), calls=%async_computation.3 | async-start | bytes 3145728 | tf_op jit(solution)/shard_map/all_to_all | solution.py:17
  99.7 0.7 copy-start.5
  114.0 48.5 %copy-start.6 = (f32[256]{0:T(256)S(1)}, f32[256]{0:T(256)}, u32[]{:S(2)}) copy-start(f32[256]{0:T(256)} %param.14) | copy-start | bytes 3076
  114.0 22.3 %all-to-all-start.4 = ((bf16[16,16,256]{2,1,0:T(8,128)(2,1)}), bf16[16,16,256]{2,1,0:T(8,128)(2,1)S(1)}, u32[]{:S(2)}, u32[]{:S(2)}) async-start(bf16[16,16,256]{2,1,0:T(8,128)(2,1)} %pad_maximum_fusion.1), calls=%async_computation.4 | async-start | bytes 262144 | tf_op jit(solution)/shard_map/all_to_all | solution.py:17
  146.9 15.3 %all-to-all-start.5 = ((bf16[16,16,128]{2,1,0:T(8,128)(2,1)}), bf16[16,16,128]{2,1,0:T(8,128)(2,1)S(1)}, u32[]{:S(2)}, u32[]{:S(2)}) async-start(bf16[16,16,128]{2,1,0:T(8,128)(2,1)} %constant_dynamic-update-slice_fusion), calls=%async_computation.5 | async-start | bytes 131072 | tf_op jit(solution)/shard_map/all_to_all | solution.py:17

commit v2 on v1

v2 whole, which is shorter than its diff:
```python
import jax
import jax.numpy as jnp
from jax import lax
from jax.experimental import pallas as pl
from jax.experimental.pallas import tpu as pltpu
from jax.sharding import Mesh
from jax.sharding import PartitionSpec as P


KEY_DIM = 128
VAL_DIM = 128
YT = ("y", "tp")
LANES = 128

eps_norm = 1e-06
f32 = jnp.float32
bf16 = jnp.bfloat16


def exchanged(value, axis):
    return lax.all_to_all(value, axis, 0, 0, tiled=True)


def copies(value, count):
    return jnp.broadcast_to(value[None], (count, *value.shape))


def call(kernel, out, flops, *args):
    outs = out if isinstance(out, (list, tuple)) else (out,)
    moved = sum(a.size * a.dtype.itemsize for a in args) + sum(o.size * o.dtype.itemsize for o in outs)
    return pl.pallas_call(
        kernel,
        out_shape=out,
        in_specs=[pl.BlockSpec(memory_space=pltpu.VMEM)] * len(args),
        out_specs=jax.tree.map(lambda _: pl.BlockSpec(memory_space=pltpu.VMEM), out),
        cost_estimate=pl.CostEstimate(flops=flops, bytes_accessed=moved, transcendentals=0),
        compiler_params=pltpu.CompilerParams(vmem_limit_bytes=16 * 1024 * 1024),
    )(*args)


def dot(a, b, dims):
    return lax.dot_general(a, b, (dims, ((), ())), preferred_element_type=f32)


def shuffled(blocks, chunk, source, rows):
    lane = lax.broadcasted_iota(jnp.int32, (rows, LANES), 1)
    result = None
    for j in range(LANES // chunk):
        block, group = source(j)
        shift = ((j - group) * chunk) % LANES
        moved = blocks(block)
        if shift:
            moved = pltpu.roll(moved, shift, 1)
        result = moved if result is None else jnp.where(lane >= j * chunk, moved, result)
    return result


def normalize_kernel(ny, nt, chunk, x_ref, gain_ref, out_ref):
    per = LANES // chunk
    rows, width = x_ref.shape
    x = x_ref[...].astype(f32)
    scale = lax.rsqrt(jnp.mean(x * x, axis=-1, keepdims=True) + eps_norm)
    normed = (x * scale * gain_ref[...]).astype(bf16).astype(f32)
    part = width // ny
    for y in range(ny):
        for q in range(part // LANES):

            def source(j):
                flat = ((q * per + j) * ny + y) * chunk
                return flat // LANES, (flat % LANES) // chunk

            block = shuffled(lambda b: normed[:, b * LANES : (b + 1) * LANES], chunk, source, rows).astype(bf16)
            for t in range(nt):
                out_ref[y, t, :, q * LANES : (q + 1) * LANES] = block


def split_parts(value):
    first = value.astype(bf16)
    rest = value - first.astype(f32)
    second = rest.astype(bf16)
    third = (rest - second.astype(f32)).astype(bf16)
    return first, second, third


def gates_kernel(fv_ref, gap_ref, piece_ref, sums_ref, inkey_ref, values_ref):
    ny, stretch, _ = fv_ref.shape
    width = gap_ref.shape[1]
    _, piece_rows, _ = piece_ref.shape
    mine = piece_rows - 8

    def total(lower):
        result = fv_ref[0, :, lower : lower + width].astype(f32)
        for k in range(1, ny):
            result = result + fv_ref[k, :, lower : lower + width].astype(f32)
        return result.astype(bf16)

    forget = total(0).astype(f32)
    values = total(width)
    values_ref[...] = values
    inkey = gap_ref[...] * jax.nn.sigmoid(-forget)
    log_forget = jnp.log1p(-inkey)
    row = lax.broadcasted_iota(jnp.int32, (stretch, stretch), 0)
    column = lax.broadcasted_iota(jnp.int32, (stretch, stretch), 1)
    causal = (row >= column).astype(bf16)
    parts = split_parts(log_forget)
    cumulative = sum(dot(causal, p, ((1,), (0,))) for p in parts)
    final = cumulative[stretch - 1 : stretch, :]
    sums_ref[...] = cumulative
    inkey_ref[...] = inkey
    key_final = (inkey * jnp.exp(final - cumulative)).astype(bf16)
    ones = jnp.ones((stretch, LANES), bf16)
    lane = lax.broadcasted_iota(jnp.int32, (8, LANES), 1)
    per_head = KEY_DIM // mine
    for h in range(width // KEY_DIM):
        cut = slice(h * KEY_DIM, (h + 1) * KEY_DIM)
        state = dot(key_final[:, cut], values[:, cut], ((0,), (0,))).astype(bf16)
        decay = jnp.exp(sum(dot(p[:, cut], ones, ((0,), (0,))) for p in parts))
        high = decay.astype(bf16).astype(f32)
        low = (decay - high).astype(bf16).astype(f32)
        for k in range(per_head):
            at = h * per_head + k
            lower = k * mine
            piece_ref[at, :mine, :] = state[lower : lower + mine]
            top = jnp.where(lane < 32, high[lower : lower + 8], low[lower : lower + 8])
            bottom = jnp.where(lane < 96, high[lower + 8 : lower + 16], low[lower + 8 : lower + 16])
            piece_ref[at, mine:, :] = jnp.where(lane < 64, top, bottom).astype(bf16)


def keys_kernel(sums_ref, inkey_ref, keys_ref):
    keys_ref[...] = (inkey_ref[...] * jnp.exp(-sums_ref[...])).astype(bf16)


def reach_kernel(sums_ref, reach_ref):
    reach_ref[...] = jnp.exp(sums_ref[...])


def prefix_kernel(piece_ref, out_ref):
    nz, mine, _ = out_ref.shape
    state = [jnp.zeros((8, VAL_DIM), f32) for _ in range(2)]
    for k in range(nz):
        out_ref[k] = jnp.concatenate(state, axis=0).astype(bf16)
        packed = piece_ref[k, mine:, :].astype(f32)
        added = piece_ref[k, :mine, :].astype(f32)
        for i in range(2):
            factor = packed[:, 64 * i : 64 * i + 1] + packed[:, 64 * i + 32 : 64 * i + 33]
            state[i] = factor * state[i] + added[8 * i : 8 * i + 8]


def inside_kernel(later_ref, reach_ref, keys_ref, values_ref, scaled_ref, inside_ref):
    ny = later_ref.shape[0]
    stretch, width = reach_ref.shape
    query = later_ref[0, :stretch, :].astype(f32)
    for k in range(1, ny):
        query = query + later_ref[k, :stretch, :].astype(f32)
    query = jax.nn.silu(query.astype(bf16).astype(f32))
    scaled = (query * reach_ref[...]).astype(bf16)
    scaled_ref[...] = scaled
    row = lax.broadcasted_iota(jnp.int32, (stretch, stretch), 0)
    column = lax.broadcasted_iota(jnp.int32, (stretch, stretch), 1)
    causal = row >= column
    for h in range(width // KEY_DIM):
        cut = slice(h * KEY_DIM, (h + 1) * KEY_DIM)
        scores = dot(scaled[:, cut], keys_ref[:, cut], ((1,), (1,)))
        scores = jnp.where(causal, scores, 0.0).astype(bf16)
        inside_ref[:, cut] = dot(scores, values_ref[:, cut], ((1,), (0,)))


def readout_kernel(later_ref, scaled_ref, inside_ref, state_ref, gain_ref, out_ref):
    ny = later_ref.shape[0]
    stretch, width = scaled_ref.shape
    hidden = []
    for h in range(width // KEY_DIM):
        cut = slice(h * KEY_DIM, (h + 1) * KEY_DIM)
        recurrent = inside_ref[:, cut] + dot(scaled_ref[:, cut], state_ref[cut, :], ((1,), (0,)))
        mean_square = jnp.mean(recurrent * recurrent, axis=-1, keepdims=True)
        hidden.append((recurrent * lax.rsqrt(mean_square + eps_norm) * gain_ref[:, cut]).astype(bf16))
    hidden = jnp.concatenate(hidden, axis=1)
    part = out_ref.shape[1] // ny
    for k in range(ny):
        out_ref[:, k * part : (k + 1) * part] = dot(hidden, later_ref[k, stretch:, :], ((1,), (1,))).astype(bf16)


def gather_kernel(nz, chunk, in_ref, out_ref):
    seqs, nt, pos, width = in_ref.shape
    ny = width // (nz * chunk)
    part = nz * chunk
    per = LANES // chunk
    for s in range(seqs):
        summed = in_ref[s, 0].astype(f32)
        for t in range(1, nt):
            summed = summed + in_ref[s, t].astype(f32)
        for b in range(width // LANES):

            def source(j):
                z, y = divmod(b * per + j, ny)
                flat = y * part + z * chunk
                return flat // LANES, (flat % LANES) // chunk

            block = shuffled(lambda k: summed[:, k * LANES : (k + 1) * LANES], chunk, source, pos)
            out_ref[s, :, b * LANES : (b + 1) * LANES] = block.astype(bf16)


def block(tokens, norm_gain, w_query, w_forget, w_value, floor_gap, head_gain, w_out):
    nz, ny, nt = (lax.axis_size(a) for a in ("z", "y", "tp"))
    pos, seqs, width = tokens.shape
    chunk, key_width = w_query.shape
    stretch = pos * ny * nt
    part = nz * chunk
    shape = jax.ShapeDtypeStruct

    ordered = tokens.transpose(1, 0, 2).reshape(seqs * pos, width)
    send = call(
        lambda *refs: normalize_kernel(ny, nt, chunk, *refs),
        shape((ny, nt, seqs * pos, part), bf16),
        1_000_000,
        ordered,
        norm_gain.reshape(1, width),
    )
    rows = exchanged(send.reshape(ny * nt, seqs, pos, part), YT)

    weights = jnp.concatenate((w_forget, w_value, w_query), axis=1)
    weights = lax.all_gather(weights, "z", axis=0, tiled=True)
    rows = rows.transpose(1, 0, 2, 3).reshape(seqs, stretch, part)

    def project(lower, upper):
        return jnp.einsum("sph,hd->spd", rows, weights[:, lower:upper], preferred_element_type=f32).astype(bf16)

    fv = exchanged(project(0, 2 * key_width), "y")
    out_z = exchanged(copies(w_out.T, nz), "z").reshape(part, key_width)
    later = jnp.concatenate((project(2 * key_width, 3 * key_width), copies(out_z, ny)), axis=1)
    later = exchanged(later, "y")

    mine = key_width // nz
    pieces, sums, inkey, values = call(
        gates_kernel,
        [
            shape((nz, mine + 8, VAL_DIM), bf16),
            shape((stretch, key_width), f32),
            shape((stretch, key_width), f32),
            shape((stretch, key_width), bf16),
        ],
        100_000_000,
        fv,
        floor_gap.reshape(1, key_width),
    )
    pieces = exchanged(pieces, "z")
    entering = call(prefix_kernel, shape((nz, mine, VAL_DIM), bf16), 1_000_000, pieces)
    incoming = exchanged(entering, "z").reshape(key_width, VAL_DIM)

    keys = call(keys_kernel, shape((stretch, key_width), bf16), 1_000_000, sums, inkey)
    reach = call(reach_kernel, shape((stretch, key_width), f32), 1_000_000, sums)
    scaled, inside = call(
        inside_kernel,
        [shape((stretch, key_width), bf16), shape((stretch, key_width), f32)],
        100_000_000,
        later,
        reach,
        keys,
        values,
    )
    mixed = call(
        readout_kernel,
        shape((stretch, width), bf16),
        300_000_000,
        later,
        scaled,
        inside,
        incoming,
        head_gain.reshape(1, key_width),
    )
    mixed = exchanged(mixed.reshape(ny * nt, pos, width), YT)
    mixed = call(
        lambda *refs: gather_kernel(nz, chunk, *refs),
        shape((seqs, pos, width), bf16),
        1_000_000,
        mixed.reshape(seqs, nt, pos, width),
    )
    return mixed.transpose(1, 0, 2)


def solution(mesh):
    finer = Mesh(mesh.devices.reshape(16, 4, mesh.shape["tp"]), ("z", "y", "tp"))
    sp = ("z", "y")
    in_specs = (
        P(("z", "y", "tp"), None, None),
        P(),
        P(sp, "tp"),
        P(sp, "tp"),
        P(sp, "tp"),
        P("tp"),
        P("tp"),
        P("tp", sp),
    )
    out_specs = P(("z", "y", "tp"), None, None)
    return jax.shard_map(block, mesh=finer, in_specs=in_specs, out_specs=out_specs, check_vma=False)
```

time: 200 us -> 167 us (0.83)
  blocking collectives: 95.8 us -> 80.4 us
  other arithmetic: 15.6 us -> 1.29 us
  Pallas kernels: 0 us -> 5.26 us
  local copies, waits for them, and re-layouts: 9.05 us -> 4.16 us
  starting transfers between devices: 34.9 us -> 30.1 us
    all_to_all x2, blocking collectives: 59.5 us -> 48.5 us  [exchanged(): return lax.all_to_all(value, axis, 0, 0, tiled=True)]
    unnamed x14 -> x0, other arithmetic: 9.3 us -> none
    pallas_call x0 -> x8, Pallas kernels: none -> 5.26 us  [call(): pl.pallas_call(kernel, out_shape=out, in_specs=[pl.BlockSpec(memory_space...]
    all_to_all x5, starting transfers between devices: 34.9 us -> 30.1 us  [exchanged(): return lax.all_to_all(value, axis, 0, 0, tiled=True)]
    all_gather x1, blocking collectives: 36.3 us -> 31.9 us  [block(): weights = lax.all_gather(weights, 'z', axis=0, tiled=True)]
    reshape x6 -> x0, local copies, waits for them, and re-layouts: 3.01 us -> none  [the longest x2 1.45 us: body(): return mixed.reshape(pos, seqs, width)]
    slice x6 -> x0, local copies, waits for them, and re-layouts: 2.44 us -> none  [the longest x1 1.15 us: body(): partial[..., :2 * key_width]]
  transfers between devices with their start and end apart: 5 -> 5, of which waited for: 4 -> 4; matrix products, arithmetic and copies ran while one was open for 3% -> 2% of each run, Pallas kernels for 0% -> 2%
where the time goes in v2:
time: 167 us; the launch traced here: 166 us
  blocking collectives  80.4 us (48%)
  waiting for transfers between devices  42.8 us (26%)
  starting transfers between devices  30.1 us (18%)
  Pallas kernels  5.26 us (3%)
  local copies, waits for them, and re-layouts  4.16 us (2%)
  matrix products  2.09 us (1%)
    all_to_all x2, blocking collectives, exchanged(): return lax.all_to_all(value, axis, 0, 0, tiled=True)  48.5 us
    all_to_all x5, waiting for transfers between devices, exchanged(): return lax.all_to_all(value, axis, 0, 0, tiled=True)  42.8 us
    all_gather x1, blocking collectives, block(): weights = lax.all_gather(weights, 'z', axis=0, tiled=True)  31.9 us
    all_to_all x5, starting transfers between devices, exchanged(): return lax.all_to_all(value, axis, 0, 0, tiled=True)  30.1 us
    pallas_call x8, Pallas kernels, call(): pl.pallas_call(kernel, out_shape=out, in_specs=[pl.BlockSpec(memory_space...  5.26 us
  transfers between devices with their start and end apart: 5, of which 4 were waited for; matrix products, arithmetic and copies ran while one was open for 2% of the time, Pallas kernels for 2%

profile of v2, /device:TPU:1, one launch (start us, length us, event | category | flops | bytes accessed | tf_op | source)
XLA Modules:
  0.0 166.3 jit_solution(13527192263545120438)
XLA Ops:
  0.0 1.0 copy.21
  1.0 0.0 copy-start
  1.0 0.7 copy-done
  1.7 0.0 copy-start.5
  1.7 0.0 copy-start.6
  1.7 0.0 copy-start.7
  1.7 1.3 shard_map.82
  3.0 10.4 %all-to-all-start = ((bf16[32,4,8,512]{3,2,1,0:T(8,128)(2,1)}), bf16[32,4,8,512]{3,2,1,0:T(8,128)(2,1)S(1)}, u32[]{:S(2)}, u32[]{:S(2)}) async-start(bf16[32,4,8,512]{3,2,1,0:T(8,128)(2,1)} %bitcast.3), calls=%async_computation | async-start | bytes 2097152 | tf_op jit(solution)/shard_map/all_to_all | solution.py:21
  13.4 0.0 copy-done.5
  13.4 0.0 copy-done.6
  13.4 0.0 copy-done.7
  13.5 31.9 %all_gather.3 = bf16[512,768]{1,0:T(8,128)(2,1)S(1)} all-gather(bf16[32,768]{1,0:T(8,128)(2,1)S(1)} %pad_maximum_fusion.1), channel_id=1, replica_groups=mesh['z'=16,'y'=4,'tp'=8] {'z'}, dimensions={0}, use_global_device_ids=true | all-gather | bytes 835584 | tf_op jit(solution)/shard_map/all_gather | solution.py:222
  45.4 0.0 copy-start.3
  45.4 0.0 all-to-all-done
  45.4 0.9 copy-done.3
  46.3 0.7 convolution_convert_fusion
  47.0 0.0 copy-start.4
  47.0 0.0 copy-start.1
  47.0 14.0 %all_to_all.35.fv_ref = bf16[4,256,512]{2,1,0:T(8,128)(2,1)S(1)} all-to-all(bf16[4,256,512]{2,1,0:T(8,128)(2,1)S(1)} %convolution_convert_fusion), channel_id=1, replica_groups=mesh['z'=16,'y'=4,'tp'=8] {'y'}, dimensions={0} | all-to-all | bytes 2097152 | tf_op jit(solution)/shard_map/all_to_all | solution.py:21
  61.0 0.0 copy-done.4
  61.0 0.7 broadcast_in_dim.6
  61.7 6.5 %all-to-all-start.1 = ((bf16[16,32,256]{2,1,0:T(8,128)(2,1)}), bf16[16,32,256]{2,1,0:T(8,128)(2,1)S(1)}, u32[]{:S(2)}, u32[]{:S(2)}) async-start(bf16[16,32,256]{2,1,0:T(8,128)(2,1)} %broadcast_in_dim.6), calls=%async_computation.1 | async-start | bytes 524288 | tf_op jit(solution)/shard_map/all_to_all | solution.py:21
  68.2 0.0 copy-done.1
  68.2 1.6 shard_map.83
  69.9 11.1 %all-to-all-done.1 = bf16[16,32,256]{2,1,0:T(8,128)(2,1)S(1)} async-done(((bf16[16,32,256]{2,1,0:T(8,128)(2,1)}), bf16[16,32,256]{2,1,0:T(8,128)(2,1)S(1)}, u32[]{:S(2)}, u32[]{:S(2)}) %all-to-all-start.1) | async-done | bytes 262176 | tf_op jit(solution)/shard_map/all_to_all | solution.py:21
  81.0 6.1 %all-to-all-start.4 = ((bf16[16,24,128]{2,1,0:T(8,128)(2,1)}), bf16[16,24,128]{2,1,0:T(8,128)(2,1)S(1)}, u32[]{:S(2)}, u32[]{:S(2)}) async-start(bf16[16,24,128]{2,1,0:T(8,128)(2,1)} %get-tuple-element.16), calls=%async_computation.4 | async-start | bytes 196608 | tf_op jit(solution)/shard_map/all_to_all | solution.py:21
  87.1 1.4 convolution_convert_fusion.1
  88.4 0.1 broadcast_in_dim.15
  88.5 1.3 pad_maximum_fusion
  89.8 9.1 %all-to-all-done.4.piece_ref = bf16[16,24,128]{2,1,0:T(8,128)(2,1)S(1)} async-done(((bf16[16,24,128]{2,1,0:T(8,128)(2,1)}), bf16[16,24,128]{2,1,0:T(8,128)(2,1)S(1)}, u32[]{:S(2)}, u32[]{:S(2)}) %all-to-all-start.4) | async-done | bytes 98336 | tf_op jit(solution)/shard_map/all_to_all | solution.py:21
  98.9 3.6 %all-to-all-start.2 = ((bf16[4,768,256]{2,1,0:T(8,128)(2,1)}), bf16[4,768,256]{2,1,0:T(8,128)(2,1)S(1)}, u32[]{:S(2)}, u32[]{:S(2)}) async-start(bf16[4,768,256]{2,1,0:T(8,128)(2,1)} %pad_maximum_fusion), calls=%async_computation.2 | async-start | bytes 3145728 | tf_op jit(solution)/shard_map/all_to_all | solution.py:21
  102.5 0.8 shard_map.87
  103.3 11.7 %all-to-all-done.2.later_ref = bf16[4,768,256]{2,1,0:T(8,128)(2,1)S(1)} async-done(((bf16[4,768,256]{2,1,0:T(8,128)(2,1)}), bf16[4,768,256]{2,1,0:T(8,128)(2,1)S(1)}, u32[]{:S(2)}, u32[]{:S(2)}) %all-to-all-start.2) | async-done | bytes 1572896 | tf_op jit(solution)/shard_map/all_to_all | solution.py:21
  115.0 3.5 %all-to-all-start.5 = ((bf16[16,16,128]{2,1,0:T(8,128)(2,1)}), bf16[16,16,128]{2,1,0:T(8,128)(2,1)S(1)}, u32[]{:S(2)}, u32[]{:S(2)}) async-start(bf16[16,16,128]{2,1,0:T(8,128)(2,1)} %shard_map.87), calls=%async_computation.5 | async-start | bytes 131072 | tf_op jit(solution)/shard_map/all_to_all | solution.py:21
  118.5 0.0 copy-start.2
  118.6 0.5 shard_map.86
  119.1 11.0 %all-to-all-done.5 = bf16[16,16,128]{2,1,0:T(8,128)(2,1)S(1)} async-done(((bf16[16,16,128]{2,1,0:T(8,128)(2,1)}), bf16[16,16,128]{2,1,0:T(8,128)(2,1)S(1)}, u32[]{:S(2)}, u32[]{:S(2)}) %all-to-all-start.5) | async-done | bytes 65568 | tf_op jit(solution)/shard_map/all_to_all | solution.py:21
  130.1 0.0 copy-done.2
  130.1 0.6 shard_map.88
  130.8 34.5 %all_to_all.36 = bf16[32,8,2048]{2,1,0:T(8,128)(2,1)S(1)} all-to-all(bf16[32,8,2048]{2,1,0:T(8,128)(2,1)S(1)} %bitcast.32), channel_id=1, replica_groups=mesh['z'=16,'y'=4,'tp'=8] {'y','tp'}, dimensions={0} | all-to-all | bytes 2097152 | tf_op jit(solution)/shard_map/all_to_all | solution.py:21
  165.3 0.2 shard_map.89
  165.5 0.8 copy.11
  (3 shorter events, 0.1 us)
Async XLA Ops:
  1.0 0.7 copy-start
  1.7 11.7 %copy-start.5 = (bf16[32,256]{1,0:T(8,128)(2,1)S(1)}, bf16[32,256]{1,0:T(8,128)(2,1)}, u32[]{:S(2)}) copy-start(bf16[32,256]{1,0:T(8,128)(2,1)} %param.10) | copy-start | bytes 49156
  1.7 11.7 %copy-start.6 = (bf16[32,256]{1,0:T(8,128)(2,1)S(1)}, bf16[32,256]{1,0:T(8,128)(2,1)}, u32[]{:S(2)}) copy-start(bf16[32,256]{1,0:T(8,128)(2,1)} %param.12) | copy-start | bytes 49156
  1.7 11.8 %copy-start.7 = (bf16[32,256]{1,0:T(8,128)(2,1)S(1)}, bf16[32,256]{1,0:T(8,128)(2,1)}, u32[]{:S(2)}) copy-start(bf16[32,256]{1,0:T(8,128)(2,1)} %param.11) | copy-start | bytes 49156
  3.0 42.4 %all-to-all-start = ((bf16[32,4,8,512]{3,2,1,0:T(8,128)(2,1)}), bf16[32,4,8,512]{3,2,1,0:T(8,128)(2,1)S(1)}, u32[]{:S(2)}, u32[]{:S(2)}) async-start(bf16[32,4,8,512]{3,2,1,0:T(8,128)(2,1)} %bitcast.3), calls=%async_computation | async-start | bytes 2097152 | tf_op jit(solution)/shard_map/all_to_all | solution.py:21
  45.4 0.9 copy-start.3
  47.0 14.0 %copy-start.4 = (bf16[256,32]{0,1:T(8,128)(2,1)S(1)}, bf16[256,32]{0,1:T(8,128)(2,1)}, u32[]{:S(2)}) copy-start(bf16[256,32]{0,1:T(8,128)(2,1)} %param.15) | copy-start | bytes 49156
  47.0 21.2 %copy-start.1 = (f32[256]{0:T(256)S(1)}, f32[256]{0:T(256)}, u32[]{:S(2)}) copy-start(f32[256]{0:T(256)} %param.13) | copy-start | bytes 3076
  61.7 19.2 %all-to-all-start.1 = ((bf16[16,32,256]{2,1,0:T(8,128)(2,1)}), bf16[16,32,256]{2,1,0:T(8,128)(2,1)S(1)}, u32[]{:S(2)}, u32[]{:S(2)}) async-start(bf16[16,32,256]{2,1,0:T(8,128)(2,1)} %broadcast_in_dim.6), calls=%async_computation.1 | async-start | bytes 524288 | tf_op jit(solution)/shard_map/all_to_all | solution.py:21
  81.0 17.9 %all-to-all-start.4 = ((bf16[16,24,128]{2,1,0:T(8,128)(2,1)}), bf16[16,24,128]{2,1,0:T(8,128)(2,1)S(1)}, u32[]{:S(2)}, u32[]{:S(2)}) async-start(bf16[16,24,128]{2,1,0:T(8,128)(2,1)} %get-tuple-element.16), calls=%async_computation.4 | async-start | bytes 196608 | tf_op jit(solution)/shard_map/all_to_all | solution.py:21
  98.9 16.1 %all-to-all-start.2 = ((bf16[4,768,256]{2,1,0:T(8,128)(2,1)}), bf16[4,768,256]{2,1,0:T(8,128)(2,1)S(1)}, u32[]{:S(2)}, u32[]{:S(2)}) async-start(bf16[4,768,256]{2,1,0:T(8,128)(2,1)} %pad_maximum_fusion), calls=%async_computation.2 | async-start | bytes 3145728 | tf_op jit(solution)/shard_map/all_to_all | solution.py:21
  115.0 15.1 %all-to-all-start.5 = ((bf16[16,16,128]{2,1,0:T(8,128)(2,1)}), bf16[16,16,128]{2,1,0:T(8,128)(2,1)S(1)}, u32[]{:S(2)}, u32[]{:S(2)}) async-start(bf16[16,16,128]{2,1,0:T(8,128)(2,1)} %shard_map.87), calls=%async_computation.5 | async-start | bytes 131072 | tf_op jit(solution)/shard_map/all_to_all | solution.py:21
  118.5 11.6 %copy-start.2 = (f32[256]{0:T(256)S(1)}, f32[256]{0:T(256)}, u32[]{:S(2)}) copy-start(f32[256]{0:T(256)} %param.14) | copy-start | bytes 3076
